TPU v7x, 512 devices: a whole 4x8x8 slice. The times are simulated.
512 devices in a mesh: gr: 2 (over z_hi), fs: 32 (over z_lo, y), tp: 8 (over x, core).
Axes of the slice: x: 4, y: 8, z: 8 (z_hi: 2, z_lo: 4; z = z_hi * 4 + z_lo), core: 2. Of those that a mesh axis runs over, the one named last changes fastest.
Arguments:
- prompt: bfloat16 [20480, 2048], P(('gr', 'fs'), 'tp'), may hold values from -6 to 6
- norm_gain: float32 [2048], P(('gr', 'fs')), may hold values from 0.1 to 1.9
- gate_weight: float32 [32, 2048, 2048], P(None, ('gr', 'fs'), 'tp'), may hold values from -0.125 to 0.125
- up_weight: float32 [32, 2048, 2048], P(None, ('gr', 'fs'), 'tp'), may hold values from -0.125 to 0.125
- down_weight: float32 [32, 2048, 2048], P(None, ('gr', 'fs'), 'tp'), may hold values from -0.125 to 0.125
- routes: int32 [20480, 2], P(('gr', 'fs')), may hold values from 0 to 31, as said below
- route_weight: float32 [20480, 2], P(('gr', 'fs')), may hold values from 0.2 to 1
Outputs:
- gate_new: bfloat16 [32, 2048, 2048], P('fs', None, 'tp')
- up_new: bfloat16 [32, 2048, 2048], P('fs', None, 'tp')
- down_new: bfloat16 [32, 2048, 2048], P('fs', 'tp')
- mixed: bfloat16 [20480, 2048], P(('gr', 'fs'), 'tp')
Inputs may be any that keep to these rules, and one draw needn't show every extreme that they name: `routes`: each row names two different experts of the same group; expert e belongs to group e // 8. Among the 320 rows of one index of gr and fs no expert is named more than 30 times, and in every draw every expert of one group is named exactly 30 times by the rows of every index.
All inputs are finite; a program needn't handle non-finite values.
Results may differ from a plain program's by a relative error of at most 0.015.
Values may be sent and summed in bfloat16 or wider, within the bound.
No kernel may reach another device: no remote copies, remote signals or barrier semaphores. Data moves between devices by JAX's collectives and lax.ppermute only.
A program may use at most 64 MiB of HBM per device.

v0:
```python
import jax
import jax.numpy as jnp
from jax import lax
from jax.sharding import PartitionSpec as P

CAP = 30


def side_by_side(arrays, axis, split_dim, concat_dim, along):
    widths = [a.shape[along] for a in arrays]
    both = jnp.concatenate(arrays, axis=along)
    whole = lax.all_to_all(both, axis, split_axis=split_dim, concat_axis=concat_dim, tiled=True)
    return tuple(jnp.split(whole, [sum(widths[:k]) for k in range(1, len(widths))], axis=along))


def side_by_side_2(arrays, axis, dim, along):
    ends, at = ([], 0)
    for a in arrays[:-1]:
        at += a.shape[along]
        ends.append(at)
    both = jnp.concatenate(arrays, axis=along)
    return tuple(jnp.split(lax.all_gather(both, axis, axis=dim, tiled=True), ends, axis=along))


def copy_for_each(array, axis):
    length = lax.axis_size(axis)
    return lax.all_to_all(
        jnp.broadcast_to(array[None], (length, *array.shape)), axis, 0, 0, tiled=True
    )


def over_copies(array, axis):
    everything = copy_for_each(array, axis)
    return jnp.sum(everything, axis=0)


def body(prompt, norm_gain, gate_weight, up_weight, down_weight, routes, route_weight):
    groups_fs = lax.axis_size("fs")
    groups_tp = lax.axis_size("tp")
    gate_cast = (gate_weight * norm_gain[None, :, None]).astype(jnp.bfloat16)
    up_cast = (up_weight * norm_gain[None, :, None]).astype(jnp.bfloat16)
    down_cast = down_weight.astype(jnp.bfloat16)
    spread = side_by_side((gate_cast, up_cast, down_cast), "fs", 0, 1, 2)
    gate_new, up_new, down_rows = side_by_side_2((spread[0], spread[1], spread[2]), "gr", 1, 0)
    down_new = lax.all_to_all(down_rows, "tp", split_axis=1, concat_axis=2, tiled=True)
    values = prompt.astype(jnp.float32)
    tok_count = prompt.shape[0]
    col_width = prompt.shape[1]
    full_width = col_width * groups_tp
    squares = jnp.sum(values * values, axis=-1, keepdims=True)
    total_squares = over_copies(squares, "tp")
    normed = (values * lax.rsqrt(total_squares / full_width + 1e-06)).astype(jnp.bfloat16)
    expert_total = gate_weight.shape[0]
    per_device = expert_total // groups_fs
    slots_all = expert_total * CAP
    picks_flat = routes.reshape(-1)
    matches = (picks_flat[:, None] == jnp.arange(expert_total, dtype=jnp.int32)[None, :]).astype(
        jnp.int32
    )
    earlier = jnp.cumsum(matches, axis=0) - matches
    slot_of = jnp.sum(earlier * matches, axis=1)
    target = (picks_flat * CAP + slot_of).reshape(tok_count, 2)
    slot_ids = jnp.arange(slots_all, dtype=jnp.int32)[None, :]
    select_first = (target[:, 0:1] == slot_ids).astype(jnp.bfloat16)
    select_second = (target[:, 1:2] == slot_ids).astype(jnp.bfloat16)
    select_both = select_first + select_second
    outbound = jnp.einsum("ts,td->sd", select_both, normed, preferred_element_type=jnp.float32)
    outbound = outbound.astype(jnp.bfloat16).reshape(groups_fs, per_device, CAP, col_width)
    moved_cols = lax.all_to_all(outbound, "fs", split_axis=0, concat_axis=0, tiled=True)
    arrived_rows = lax.all_gather(moved_cols, "tp", axis=3, tiled=True)
    gate_pre = jnp.einsum(
        "sxcd,xdh->sxch", arrived_rows, gate_new, preferred_element_type=jnp.float32
    )
    up_pre = jnp.einsum("sxcd,xdh->sxch", arrived_rows, up_new, preferred_element_type=jnp.float32)
    hidden = (jax.nn.silu(gate_pre) * up_pre).astype(jnp.bfloat16)
    partial_value = jnp.einsum(
        "sxch,xhd->sxcd", hidden, down_new, preferred_element_type=jnp.float32
    )
    summed = lax.psum_scatter(
        partial_value.astype(jnp.bfloat16), "tp", scatter_dimension=3, tiled=True
    )
    returned = lax.all_to_all(summed, "fs", split_axis=0, concat_axis=0, tiled=True)
    returned_flat = returned.reshape(slots_all, returned.shape[3])
    pick_first = jnp.dot(select_first, returned_flat, preferred_element_type=jnp.float32)
    pick_second = jnp.dot(select_second, returned_flat, preferred_element_type=jnp.float32)
    mixed = route_weight[:, 0:1] * pick_first + route_weight[:, 1:2] * pick_second
    return (gate_new, up_new, down_new, mixed.astype(jnp.bfloat16))


def solution(mesh):
    return jax.shard_map(
        body,
        mesh=mesh,
        in_specs=(
            P(("gr", "fs"), "tp"),
            P(("gr", "fs")),
            P(None, ("gr", "fs"), "tp"),
            P(None, ("gr", "fs"), "tp"),
            P(None, ("gr", "fs"), "tp"),
            P(("gr", "fs"), None),
            P(("gr", "fs"), None),
        ),
        out_specs=(
            P("fs", None, "tp"),
            P("fs", None, "tp"),
            P("fs", "tp", None),
            P(("gr", "fs"), "tp"),
        ),
        check_vma=False,
    )
```

profile of v0, /device:TPU:15, one launch (start us, length us, event | category | flops | bytes accessed | tf_op | source)
XLA Modules:
  0.0 307.7 jit_solution(11874860149354385042)
XLA Ops:
  7.2 0.0 all-gather.3.cloned.1.call-start
  7.2 1.4 convert_element_type.48
  8.6 0.1 copy-done
  8.7 1.5 multiply_convert_fusion.1
  10.3 0.1 pad_maximum_fusion
  10.4 51.0 %all_to_all.45 = bf16[32,32,768]{2,1,0:T(8,128)(2,1)S(1)} all-to-all(bf16[32,32,768]{2,1,0:T(8,128)(2,1)S(1)} %pad_maximum_fusion), channel_id=1, replica_groups=mesh['gr'=2,'fs'=32,'tp'=8] {'fs'}, dimensions={0} | all-to-all | bytes 3145728 | tf_op jit(solution)/shard_map/all_to_all | solution.py:12
  61.4 0.1 fusion.55
  61.5 1.4 pad_maximum_fusion.1
  62.9 0.9 copy-done.2
  63.8 0.1 fusion.45
  63.9 0.6 broadcast_in_dim.2
  64.6 7.0 %all-to-all-start.2 = ((f32[8,320,1]{1,2,0:T(1,128)}), f32[8,320,1]{1,2,0:T(1,128)S(1)}, u32[]{:S(2)}, u32[]{:S(2)}) async-start(f32[8,320,1]{1,2,0:T(1,128)} %broadcast_in_dim.2), calls=%async_computation.2 | async-start | bytes 24576 | tf_op jit(solution)/shard_map/all_to_all | solution.py:27
  71.5 0.1 copy.66
  71.7 0.1 eq.59
  71.8 0.1 eq.55
  72.0 1.5 reduce-window.6
  73.4 0.3 slice_reduce_fusion
  73.7 0.1 fusion.51
  73.8 0.1 reduce_sum.30
  74.0 0.1 copy.69
  74.1 0.3 all-to-all-done.2
  74.5 0.7 convolution_convert_fusion
  75.2 0.1 reshape.74
  75.4 21.0 %all_to_all.46 = bf16[32,1,30,256]{3,2,1,0:T(8,128)(2,1)S(1)} all-to-all(bf16[32,1,30,256]{3,2,1,0:T(8,128)(2,1)S(1)} %bitcast.91), channel_id=1, replica_groups=mesh['gr'=2,'fs'=32,'tp'=8] {'fs'}, dimensions={0} | all-to-all | bytes 983040 | tf_op jit(solution)/shard_map/all_to_all | solution.py:69
  96.4 1.1 copy.72
  97.4 0.0 reduce-scatter.2.cloned.1.call-start
  97.5 67.4 %all-gather.3.cloned.1.call-done = bf16[3,2048,256]{2,1,0:T(8,128)(2,1)} async-done(((bf16[3,1024,256]{2,1,0:T(8,128)(2,1)}), bf16[3,2048,256]{2,1,0:T(8,128)(2,1)}) %all-gather.3.cloned.1.call-update) | async-done | bytes 3145744 | tf_op jit(solution)/shard_map/all_gather | solution.py:22
  164.9 3.4 %fusion.54 = (bf16[1,2048,256]{2,1,0:T(8,128)(2,1)S(1)}, bf16[1,2048,256]{2,1,0:T(8,128)(2,1)}, bf16[1,2048,256]{2,1,0:T(8,128)(2,1)}) fusion(bf16[3,2048,256]{2,1,0:T(8,128)(2,1)} %all-gather.3.cloned.1.call-done), kind=kLoop, calls=%fused_computation.59 | loop fusion | bytes 6291456 | tf_op jit(solution)/shard_map/split | solution.py:22
  168.3 11.6 %copy.79 = bf16[1,2048,256]{2,0,1:T(2,128)(2,1)S(1)} copy(bf16[1,2048,256]{2,1,0:T(8,128)(2,1)S(1)} %get-tuple-element.16) | data formatting | bytes 2097152 | tf_op jit(solution)/shard_map/split | solution.py:22
  179.9 0.5 broadcast.41
  180.4 10.6 %reduce.11 = bf16[2048,256]{1,0:T(8,128)(2,1)S(1)} reduce(bf16[2048,1,256]{2,1,0:T(2,128)(2,1)S(1)} %bitcast.88, bf16[]{:T(256)} %broadcast.41), dimensions={1}, to_apply=%bitcast.83.reduce_sub_computation | reduce | bytes 2097154
  191.1 0.3 reshape.88
  191.3 22.2 %all_to_all.47 = bf16[8,2,32768]{2,1,0:T(2,128)(2,1)S(1)} all-to-all(bf16[8,2,32768]{2,1,0:T(2,128)(2,1)S(1)} %reshape.88), channel_id=1, replica_groups=mesh['gr'=2,'fs'=32,'tp'=8] {'tp'}, dimensions={0} | all-to-all | bytes 2097152 | tf_op jit(solution)/shard_map/all_to_all | solution.py:45
  213.5 1.0 reshape.89
  214.6 0.2 copy.75
  214.7 0.6 copy.70
  215.3 0.5 reshape.81
  215.9 4.6 %fusion.4 = f32[32,1,30,256]{3,0,2,1:T(8,128)} fusion(bf16[32,1,30,2048]{3,0,2,1:T(8,128)(2,1)} %all-gather.5.cloned.1.call-done, bf16[1,2048,256]{2,1,0:T(8,128)(2,1)} %get-tuple-element.18), kind=kOutput, calls=%fused_computation.7 | convolution fusion | flops 1006632960 | bytes 5963776 | tf_op jit(solution)/shard_map/sxcd,xdh->sxch/dot_general | solution.py:71
  220.6 8.4 %convert_bitcast_fusion = bf16[32,1,30,2048]{3,0,2,1:T(8,128)(2,1)} fusion(bf16[256,2048,1]{1,0,2:T(8,128)(2,1)S(1)} %reshape.81, bf16[32,1,30,2048]{3,0,2,1:T(8,128)(2,1)} %all-gather.5.cloned.1.call-done, bf16[1,2048,256]{2,1,0:T(8,128)(2,1)S(1)} %copy-done.1, f32[32,1,30,256]{3,0,2,1:T(8,128)} %fusion.4), kind=kOutput, calls=%fused_computation.4 | convolution fusion | flops 2016706560 | bytes 10944512 | tf_op jit(solution)/shard_map/sxch,xhd->sxcd/dot_general | solution.py:76
  229.0 40.6 %reduce-scatter.2.cloned.1.call-done = bf16[32,1,30,256]{3,0,2,1:T(8,128)(2,1)} async-done(((bf16[32,1,30,2048]{3,0,2,1:T(8,128)(2,1)}), bf16[32,1,30,256]{3,0,2,1:T(8,128)(2,1)}) %reduce-scatter.2.cloned.1.call-update) | async-done | bytes 491536 | tf_op jit(solution)/shard_map/reduce_scatter | solution.py:79
  269.6 2.1 copy.73
  271.7 10.1 %all-to-all-start.4 = ((bf16[32,1,30,256]{3,2,1,0:T(8,128)(2,1)}), bf16[32,1,30,256]{3,2,1,0:T(8,128)(2,1)S(1)}, u32[]{:S(2)}, u32[]{:S(2)}) async-start(bf16[32,1,30,256]{3,2,1,0:T(8,128)(2,1)} %copy.73), calls=%async_computation.5 | async-start | bytes 1048576 | tf_op jit(solution)/shard_map/all_to_all | solution.py:82
  281.8 0.5 copy.65
  282.4 1.4 copy.74
  283.8 15.8 %all-to-all-done.4 = bf16[32,1,30,256]{3,2,1,0:T(8,128)(2,1)S(1)} async-done(((bf16[32,1,30,256]{3,2,1,0:T(8,128)(2,1)}), bf16[32,1,30,256]{3,2,1,0:T(8,128)(2,1)S(1)}, u32[]{:S(2)}, u32[]{:S(2)}) %all-to-all-start.4) | async-done | bytes 491552 | tf_op jit(solution)/shard_map/all_to_all | solution.py:82
  299.5 0.1 reshape.78
  299.7 0.4 fusion.23
  300.1 1.1 fusion.26
  (22 shorter events, 0.2 us)
Async XLA Ops:
  7.2 1.4 copy-start.5
  7.2 1.5 copy-start
  7.2 157.7 %all-gather.3.cloned.1.call-start = ((), (), s32[]{:S(2)}) async-start(), calls=%async_computation.6 | async-start | bytes 4718592 | tf_op jit(solution)/shard_map/all_gather | solution.py:22
  62.9 0.9 copy-start.2
  62.9 8.7 %copy-start.3 = (s32[320,2]{0,1:T(2,128)S(1)}, s32[320,2]{0,1:T(2,128)}, u32[]{:S(2)}) copy-start(s32[320,2]{0,1:T(2,128)} %param.12) | copy-start | bytes 7684
  64.6 9.9 %all-to-all-start.2 = ((f32[8,320,1]{1,2,0:T(1,128)}), f32[8,320,1]{1,2,0:T(1,128)S(1)}, u32[]{:S(2)}, u32[]{:S(2)}) async-start(f32[8,320,1]{1,2,0:T(1,128)} %broadcast_in_dim.2), calls=%async_computation.2 | async-start | bytes 24576 | tf_op jit(solution)/shard_map/all_to_all | solution.py:27
  71.5 144.4 %all-gather.5.cloned.1.call-start = ((), (), s32[]{:S(2)}) async-start(), calls=%async_computation.7 | async-start | bytes 4423680 | tf_op jit(solution)/shard_map/all_gather | solution.py:70
  97.4 172.1 %reduce-scatter.2.cloned.1.call-start = ((), (), s32[]{:S(2)}) async-start(), calls=%async_computation.8 | async-start | bytes 4423680 | tf_op jit(solution)/shard_map/reduce_scatter | solution.py:79
  215.9 4.7 %copy-start.1 = (bf16[1,2048,256]{2,1,0:T(8,128)(2,1)S(1)}, bf16[1,2048,256]{2,1,0:T(8,128)(2,1)}, u32[]{:S(2)}) copy-start(bf16[1,2048,256]{2,1,0:T(8,128)(2,1)} %get-tuple-element.17) | copy-start | bytes 3145732
  228.9 52.8 %copy-start.4 = (f32[320,2]{0,1:T(2,128)S(1)}, f32[320,2]{0,1:T(2,128)}, u32[]{:S(2)}) copy-start(f32[320,2]{0,1:T(2,128)} %param.13) | copy-start | bytes 7684
  271.7 27.9 %all-to-all-start.4 = ((bf16[32,1,30,256]{3,2,1,0:T(8,128)(2,1)}), bf16[32,1,30,256]{3,2,1,0:T(8,128)(2,1)S(1)}, u32[]{:S(2)}, u32[]{:S(2)}) async-start(bf16[32,1,30,256]{3,2,1,0:T(8,128)(2,1)} %copy.73), calls=%async_computation.5 | async-start | bytes 1048576 | tf_op jit(solution)/shard_map/all_to_all | solution.py:82
Sparse Core Ops, SparseCore 0:
  63.0 101.8 all-gather.2
  167.6 46.1 all-gather.4
  229.1 40.4 reduce-scatter.1
where the time goes:
time: 308 us
  waiting for transfers between devices  124 us (40%)
  blocking collectives  94.2 us (31%)
  local copies, waits for them, and re-layouts  26.2 us (9%)
  starting transfers between devices  17.2 us (6%)
  other arithmetic  16.8 us (5%)
  matrix products  15.1 us (5%)
  between operations  14 us (5%)
    all_gather x1, waiting for transfers between devices, side_by_side_2(): lax.all_gather(both, axis, axis=dim, tiled=True)  67.4 us
    all_to_all x1, blocking collectives, side_by_side(): lax.all_to_all(both, axis, split_axis=split_dim, concat_axis=concat_dim,...  51 us
    reduce_scatter x1, waiting for transfers between devices, body(): lax.psum_scatter(partial_value.astype(jnp.bfloat16), 'tp', scatter_dimens...  40.6 us
    all_to_all x1, blocking collectives, body(): lax.all_to_all(down_rows, 'tp', split_axis=1, concat_axis=2, tiled=True)  22.2 us
    all_to_all x1, blocking collectives, body(): lax.all_to_all(outbound, 'fs', split_axis=0, concat_axis=0, tiled=True)  21 us
    all_to_all x1, waiting for transfers between devices, body(): lax.all_to_all(summed, 'fs', split_axis=0, concat_axis=0, tiled=True)  15.8 us
    split x2, local copies, waits for them, and re-layouts, side_by_side_2(): jnp.split(lax.all_gather(both, axis, axis=dim, tiled=True), ends, axis=al...  15 us
    unnamed x1, other arithmetic  10.6 us
  transfers between devices with their start and end apart: 5, of which 4 were waited for; matrix products, arithmetic and copies ran while one was open for 12% of the time, Pallas kernels for 0%

commit v1 on v0

--- a/solution.py
+++ b/solution.py
@@ -42,7 +42,10 @@
     down_cast = down_weight.astype(jnp.bfloat16)
     spread = side_by_side((gate_cast, up_cast, down_cast), "fs", 0, 1, 2)
     gate_new, up_new, down_rows = side_by_side_2((spread[0], spread[1], spread[2]), "gr", 1, 0)
-    down_new = lax.all_to_all(down_rows, "tp", split_axis=1, concat_axis=2, tiled=True)
+    down_new = jnp.concatenate(
+        lax.all_to_all(jnp.stack(jnp.split(down_rows, lax.axis_size("tp"), axis=1)), "tp", 0, 0),
+        axis=2,
+    )
     values = prompt.astype(jnp.float32)
     tok_count = prompt.shape[0]
     col_width = prompt.shape[1]

time: 308 us -> 306 us (level)
  waiting for transfers between devices: 124 us -> 154 us
  blocking collectives: 94.2 us -> 71.9 us
  other arithmetic: 16.8 us -> 6.43 us
  starting transfers between devices: 17.2 us -> 22.4 us
  local copies, waits for them, and re-layouts: 26.2 us -> 22.3 us
    all_to_all x1 -> x0, blocking collectives: 22.2 us -> none  [body(): lax.all_to_all(down_rows, 'tp', split_axis=1, concat_axis=2, tiled=True)]
    all_to_all x0 -> x1, waiting for transfers between devices: none -> 18.5 us  [body(): lax.all_to_all(jnp.stack(jnp.split(down_rows, lax.axis_size('tp'), axis=1...]
    split x2 -> x1, local copies, waits for them, and re-layouts: 15 us -> 2.65 us  [side_by_side_2(): jnp.split(lax.all_gather(both, axis, axis=dim, tiled=True), ends, axis=al...]
    unnamed x1 -> x0, other arithmetic: 10.6 us -> none
    all_gather x1, waiting for transfers between devices: 0.02 us -> 8.38 us  [body(): arrived_rows = lax.all_gather(moved_cols, 'tp', axis=3, tiled=True)]
    unnamed x18 -> x17, local copies, waits for them, and re-layouts: 4.59 us -> 12.5 us
    all_to_all x0 -> x1, starting transfers between devices: none -> 5.28 us  [body(): lax.all_to_all(jnp.stack(jnp.split(down_rows, lax.axis_size('tp'), axis=1...]
  transfers between devices with their start and end apart: 5 -> 6, of which waited for: 4 -> 6; matrix products, arithmetic and copies ran while one was open for 12% -> 7% of each run, Pallas kernels for 0% -> 0%
where the time goes in v1:
time: 306 us; the launch traced here: 305 us
  waiting for transfers between devices  154 us (50%)
  blocking collectives  71.9 us (23%)
  starting transfers between devices  22.4 us (7%)
  local copies, waits for them, and re-layouts  22.3 us (7%)
  matrix products  13.9 us (5%)
  between operations  13.9 us (5%)
  other arithmetic  6.43 us (2%)
    all_gather x1, waiting for transfers between devices, side_by_side_2(): lax.all_gather(both, axis, axis=dim, tiled=True)  67.4 us
    all_to_all x1, blocking collectives, side_by_side(): lax.all_to_all(both, axis, split_axis=split_dim, concat_axis=concat_dim,...  51 us
    reduce_scatter x1, waiting for transfers between devices, body(): lax.psum_scatter(partial_value.astype(jnp.bfloat16), 'tp', scatter_dimens...  43.4 us
    all_to_all x1, blocking collectives, body(): lax.all_to_all(outbound, 'fs', split_axis=0, concat_axis=0, tiled=True)  20.9 us
    all_to_all x1, waiting for transfers between devices, body(): lax.all_to_all(jnp.stack(jnp.split(down_rows, lax.axis_size('tp'), axis=1...  18.5 us
    all_to_all x1, waiting for transfers between devices, body(): lax.all_to_all(summed, 'fs', split_axis=0, concat_axis=0, tiled=True)  16.3 us
    unnamed x17, local copies, waits for them, and re-layouts  12.5 us
    all_to_all x1, starting transfers between devices, body(): lax.all_to_all(summed, 'fs', split_axis=0, concat_axis=0, tiled=True)  10.1 us
  transfers between devices with their start and end apart: 6, of which 6 were waited for; matrix products, arithmetic and copies ran while one was open for 7% of the time, Pallas kernels for 0%

profile of v1, /device:TPU:15, one launch (start us, length us, event | category | flops | bytes accessed | tf_op | source)
XLA Modules:
  0.0 305.2 jit_solution(2975324531599720272)
XLA Ops:
  7.2 0.0 all-gather.3.cloned.1.call-start
  7.2 1.3 convert_element_type.48
  8.5 1.9 multiply_convert_fusion.1
  10.4 0.1 pad_maximum_fusion
  10.5 51.0 %all_to_all.32 = bf16[32,32,768]{2,1,0:T(8,128)(2,1)S(1)} all-to-all(bf16[32,32,768]{2,1,0:T(8,128)(2,1)S(1)} %pad_maximum_fusion), channel_id=1, replica_groups=mesh['gr'=2,'fs'=32,'tp'=8] {'fs'}, dimensions={0} | all-to-all | bytes 3145728 | tf_op jit(solution)/shard_map/all_to_all | solution.py:12
  61.6 0.1 fusion.63
  61.7 1.4 pad_maximum_fusion.1
  63.0 0.0 all-gather.3.cloned.1.call-update
  63.1 0.1 fusion.45
  63.2 0.6 broadcast_in_dim.2
  63.8 7.0 %all-to-all-start.2 = ((f32[8,320,1]{1,2,0:T(1,128)}), f32[8,320,1]{1,2,0:T(1,128)S(1)}, u32[]{:S(2)}, u32[]{:S(2)}) async-start(f32[8,320,1]{1,2,0:T(1,128)} %broadcast_in_dim.2), calls=%async_computation.2 | async-start | bytes 24576 | tf_op jit(solution)/shard_map/all_to_all | solution.py:27
  70.8 0.1 copy.47
  71.0 0.1 eq.59
  71.1 0.1 eq.55
  71.3 1.5 reduce-window.6
  72.7 0.3 slice_reduce_fusion
  73.0 0.1 fusion.59
  73.1 0.1 reduce_sum.30
  73.3 0.1 copy.50
  73.4 0.3 all-to-all-done.2
  73.8 0.7 convolution_convert_fusion
  74.5 0.1 reshape.82
  74.6 20.9 %all_to_all.33 = bf16[32,1,30,256]{3,2,1,0:T(8,128)(2,1)S(1)} all-to-all(bf16[32,1,30,256]{3,2,1,0:T(8,128)(2,1)S(1)} %bitcast.116), channel_id=1, replica_groups=mesh['gr'=2,'fs'=32,'tp'=8] {'fs'}, dimensions={0} | all-to-all | bytes 983040 | tf_op jit(solution)/shard_map/all_to_all | solution.py:72
  95.5 1.1 copy.53
  96.7 67.4 %all-gather.3.cloned.1.call-done = bf16[3,2048,256]{2,1,0:T(8,128)(2,1)} async-done(((bf16[3,1024,256]{2,1,0:T(8,128)(2,1)}), bf16[3,2048,256]{2,1,0:T(8,128)(2,1)}) %all-gather.3.cloned.1.call-update) | async-done | bytes 3145744 | tf_op jit(solution)/shard_map/all_gather | solution.py:22
  164.1 1.6 fusion.56
  165.7 1.6 fusion.55
  167.2 1.6 fusion.54
  168.8 1.6 fusion.53
  170.4 1.6 fusion.52
  171.9 1.6 fusion.51
  173.5 1.6 fusion.50
  175.1 1.6 fusion.49
  176.6 5.3 %all-to-all-start.1 = ((bf16[8,1,256,256]{3,2,1,0:T(8,128)(2,1)}), bf16[8,1,256,256]{3,2,1,0:T(8,128)(2,1)S(1)}, u32[]{:S(2)}, u32[]{:S(2)}) async-start(bf16[8,1,256,256]{3,2,1,0:T(8,128)(2,1)} %fusion.49), calls=%async_computation.1 | async-start | bytes 2097152 | tf_op jit(solution)/shard_map/all_to_all | solution.py:46
  181.9 2.7 fusion.62
  184.6 18.5 %all-to-all-done.1 = bf16[8,1,256,256]{3,2,1,0:T(8,128)(2,1)S(1)} async-done(((bf16[8,1,256,256]{3,2,1,0:T(8,128)(2,1)}), bf16[8,1,256,256]{3,2,1,0:T(8,128)(2,1)S(1)}, u32[]{:S(2)}, u32[]{:S(2)}) %all-to-all-start.1) | async-done | bytes 1048608 | tf_op jit(solution)/shard_map/all_to_all | solution.py:46
  203.0 0.5 copy.46
  203.6 8.4 %all-gather.5.cloned.1.call-done = bf16[32,1,30,2048]{3,0,2,1:T(8,128)(2,1)} async-done(((bf16[32,1,30,256]{3,0,2,1:T(8,128)(2,1)}), bf16[32,1,30,2048]{3,0,2,1:T(8,128)(2,1)}) %all-gather.5.cloned.1.call-update) | async-done | bytes 3932176 | tf_op jit(solution)/shard_map/all_gather | solution.py:73
  211.9 3.6 %fusion.4 = f32[32,1,30,256]{3,0,2,1:T(8,128)S(1)} fusion(bf16[32,1,30,2048]{3,0,2,1:T(8,128)(2,1)} %all-gather.5.cloned.1.call-done, bf16[1,2048,256]{2,1,0:T(8,128)(2,1)} %get-tuple-element.25), kind=kOutput, calls=%fused_computation.7 | convolution fusion | flops 1006632960 | bytes 5963776 | tf_op jit(solution)/shard_map/sxcd,xdh->sxch/dot_general | solution.py:74
  215.6 8.1 %convert_bitcast_fusion = bf16[32,1,30,2048]{3,0,2,1:T(8,128)(2,1)} fusion(bf16[256,2048,1]{0,1,2:T(8,128)(2,1)S(1)} %bitcast.113, bf16[32,1,30,2048]{3,0,2,1:T(8,128)(2,1)} %all-gather.5.cloned.1.call-done, bf16[1,2048,256]{2,1,0:T(8,128)(2,1)S(1)} %get-tuple-element.24, f32[32,1,30,256]{3,0,2,1:T(8,128)S(1)} %fusion.4), kind=kOutput, calls=%fused_computation.4 | convolution fusion | flops 2016706560 | bytes 10944512 | tf_op jit(solution)/shard_map/sxch,xhd->sxcd/dot_general | solution.py:79
  223.7 43.4 %reduce-scatter.2.cloned.1.call-done = bf16[32,1,30,256]{3,0,2,1:T(8,128)(2,1)} async-done(((bf16[32,1,30,2048]{3,0,2,1:T(8,128)(2,1)}), bf16[32,1,30,256]{3,0,2,1:T(8,128)(2,1)}) %reduce-scatter.2.cloned.1.call-update) | async-done | bytes 491536 | tf_op jit(solution)/shard_map/reduce_scatter | solution.py:82
  267.1 2.1 copy.55
  269.2 10.1 %all-to-all-start.4 = ((bf16[32,1,30,256]{3,2,1,0:T(8,128)(2,1)}), bf16[32,1,30,256]{3,2,1,0:T(8,128)(2,1)S(1)}, u32[]{:S(2)}, u32[]{:S(2)}) async-start(bf16[32,1,30,256]{3,2,1,0:T(8,128)(2,1)} %copy.55), calls=%async_computation.5 | async-start | bytes 1048576 | tf_op jit(solution)/shard_map/all_to_all | solution.py:85
  279.4 1.4 copy.56
  280.8 16.3 %all-to-all-done.4 = bf16[32,1,30,256]{3,2,1,0:T(8,128)(2,1)S(1)} async-done(((bf16[32,1,30,256]{3,2,1,0:T(8,128)(2,1)}), bf16[32,1,30,256]{3,2,1,0:T(8,128)(2,1)S(1)}, u32[]{:S(2)}, u32[]{:S(2)}) %all-to-all-start.4) | async-done | bytes 491552 | tf_op jit(solution)/shard_map/all_to_all | solution.py:85
  297.1 0.1 reshape.86
  297.2 0.4 fusion.25
  297.6 1.1 fusion.28
  (19 shorter events, 0.2 us)
Async XLA Ops:
  7.2 156.9 %all-gather.3.cloned.1.call-start = ((), (), s32[]{:S(2)}) async-start(), calls=%async_computation.6 | async-start | bytes 4718592 | tf_op jit(solution)/shard_map/all_gather | solution.py:22
  61.7 1.4 copy-start.1
  61.7 9.1 %copy-start.2 = (s32[320,2]{0,1:T(2,128)S(1)}, s32[320,2]{0,1:T(2,128)}, u32[]{:S(2)}) copy-start(s32[320,2]{0,1:T(2,128)} %param.12) | copy-start | bytes 7684
  63.8 9.9 %all-to-all-start.2 = ((f32[8,320,1]{1,2,0:T(1,128)}), f32[8,320,1]{1,2,0:T(1,128)S(1)}, u32[]{:S(2)}, u32[]{:S(2)}) async-start(f32[8,320,1]{1,2,0:T(1,128)} %broadcast_in_dim.2), calls=%async_computation.2 | async-start | bytes 24576 | tf_op jit(solution)/shard_map/all_to_all | solution.py:27
  70.8 141.1 %all-gather.5.cloned.1.call-start = ((), (), s32[]{:S(2)}) async-start(), calls=%async_computation.7 | async-start | bytes 4423680 | tf_op jit(solution)/shard_map/all_gather | solution.py:73
  176.6 26.4 %all-to-all-start.1 = ((bf16[8,1,256,256]{3,2,1,0:T(8,128)(2,1)}), bf16[8,1,256,256]{3,2,1,0:T(8,128)(2,1)S(1)}, u32[]{:S(2)}, u32[]{:S(2)}) async-start(bf16[8,1,256,256]{3,2,1,0:T(8,128)(2,1)} %fusion.49), calls=%async_computation.1 | async-start | bytes 2097152 | tf_op jit(solution)/shard_map/all_to_all | solution.py:46
  181.9 85.2 %reduce-scatter.2.cloned.1.call-start = ((), (), s32[]{:S(2)}) async-start(), calls=%async_computation.8 | async-start | bytes 4423680 | tf_op jit(solution)/shard_map/reduce_scatter | solution.py:82
  184.6 31.0 %copy-start = (bf16[1,2048,256]{2,1,0:T(8,128)(2,1)}, bf16[1,2048,256]{2,1,0:T(8,128)(2,1)S(1)}, u32[]{:S(2)}) copy-start(bf16[1,2048,256]{2,1,0:T(8,128)(2,1)S(1)} %get-tuple-element.24) | copy-start | bytes 3145732
  223.7 55.7 %copy-start.3 = (f32[320,2]{0,1:T(2,128)S(1)}, f32[320,2]{0,1:T(2,128)}, u32[]{:S(2)}) copy-start(f32[320,2]{0,1:T(2,128)} %param.13) | copy-start | bytes 7684
  269.2 27.9 %all-to-all-start.4 = ((bf16[32,1,30,256]{3,2,1,0:T(8,128)(2,1)}), bf16[32,1,30,256]{3,2,1,0:T(8,128)(2,1)S(1)}, u32[]{:S(2)}, u32[]{:S(2)}) async-start(bf16[32,1,30,256]{3,2,1,0:T(8,128)(2,1)} %copy.55), calls=%async_computation.5 | async-start | bytes 1048576 | tf_op jit(solution)/shard_map/all_to_all | solution.py:85
Sparse Core Ops, SparseCore 0:
  63.2 100.8 all-gather.2
  166.2 45.6 all-gather.4
  223.8 43.2 reduce-scatter.1
